TPU v7x, 32 devices: a whole 2x2x4 slice. The times are simulated.
32 devices in a mesh: sp: 4 (over z), fs: 4 (over y, x), tp: 2 (over core).
Axes of the slice: x: 2, y: 2, z: 4, core: 2. Of those that a mesh axis runs over, the one named last changes fastest.
Arguments:
- tokens: bfloat16 [4, 8192, 2048], P('fs', 'sp'), may hold values from -21 to 21
- norm_gain: float32 [2048], replicated, may hold values from 0.1 to 1.9
- w_query: bfloat16 [2048, 1024], P(None, 'tp'), may hold values from -0.125 to 0.125
- w_key: bfloat16 [2048, 256], P(None, 'tp'), may hold values from -0.125 to 0.125
- w_value: bfloat16 [2048, 256], P(None, 'tp'), may hold values from -0.125 to 0.125
- w_pool: bfloat16 [2048, 1024], P(None, 'tp'), may hold values from -0.125 to 0.125
- w_group: bfloat16 [4, 256, 256], P('tp'), may hold values from -0.375 to 0.375
- w_out: bfloat16 [2048, 2048], replicated, may hold values from -0.125 to 0.125
- sinks: float32 [16], P('tp'), may hold values from -1 to 260
Outputs:
- mixed: bfloat16 [4, 8192, 2048], P('fs', ('sp', 'tp'))
- log_sums: float32 [4, 16, 8192], P('fs', 'tp', 'sp')
All inputs are finite; a program needn't handle non-finite values.
Results may differ from a plain program's by a relative error of at most 0.009.
Values may be sent and summed in bfloat16 or wider, within the bound.
A program may use at most 192 MiB of HBM per device.

v0:
```python
import functools

import jax
import jax.numpy as jnp
from jax import lax
from jax.experimental import pallas as pl
from jax.experimental.pallas import tpu as pltpu
from jax.sharding import PartitionSpec as P

HEAD_SIZE = 64
GDIM = 256
WINDOW = 128
LN_EPS = 1e-05
SUB = 256
VMEM = 63 * 2**20
MESH = pl.DeviceIdType.MESH
BF = jnp.bfloat16
F32 = jnp.float32
NEG = -1e30


def dot(a, b, dims=((1,), (0,))):
    return lax.dot_general(a, b, (dims, ((), ())), preferred_element_type=F32)


def project_kernel(subs, tok, gain, wq, wk, wv, wp, q, kd, vt, pool, bsum, total):
    step = pl.program_id(0)
    width = tok.shape[1]
    rows_sums = []
    for s in range(subs):
        rows = slice(s * SUB, (s + 1) * SUB)
        x = tok[rows, :].astype(F32)
        centered = x - jnp.sum(x, axis=-1, keepdims=True) * (1.0 / width)
        variance = jnp.sum(centered * centered, axis=-1, keepdims=True) * (1.0 / width)
        normed = (centered * lax.rsqrt(variance + LN_EPS) * gain[...]).astype(BF)
        q[rows, :] = (dot(normed, wq[...]) * HEAD_SIZE**-0.5).astype(BF)
        k = dot(normed, wk[...])
        rolled = pltpu.roll(k, HEAD_SIZE, 1)
        low = lax.broadcasted_iota(jnp.int32, k.shape, 1) < HEAD_SIZE
        kd[rows, :WINDOW] = jnp.where(low, k, rolled).astype(BF)
        kd[rows, WINDOW:] = jnp.where(low, rolled, k).astype(BF)
        vt[:, rows] = dot(normed, wv[...]).T.astype(BF)
        p = dot(normed, wp[...]).astype(BF)
        pool[rows, :] = p
        pf = p.astype(F32)
        for b in range(SUB // WINDOW):
            rows_sums.append(
                jnp.sum(pf[b * WINDOW : (b + 1) * WINDOW], axis=0, keepdims=True)
            )
    tile_sum = functools.reduce(lambda a, b: a + b, rows_sums)
    pad = jnp.zeros((8 - len(rows_sums), pool.shape[1]), F32)
    bsum[0] = jnp.concatenate(rows_sums + [pad], axis=0)

    @pl.when(step == 0)
    def _():
        total[...] = tile_sum

    @pl.when(step > 0)
    def _():
        total[...] += tile_sum


def project(tokens, gain, wq, wk, wv, wp):
    length, width = tokens.shape
    tile = 512
    steps = length // tile
    qw, kw, pw = wq.shape[1], wk.shape[1], wp.shape[1]
    whole = lambda a: pl.BlockSpec(a.shape, lambda i: (0, 0), pipeline_mode=pl.Buffered(1))
    return pl.pallas_call(
        functools.partial(project_kernel, tile // SUB),
        grid=(steps,),
        in_specs=[
            pl.BlockSpec((tile, width), lambda i: (i, 0)),
            whole(gain), whole(wq), whole(wk), whole(wv), whole(wp),
        ],
        out_specs=[
            pl.BlockSpec((tile, qw), lambda i: (i, 0)),
            pl.BlockSpec((tile, 2 * kw), lambda i: (i, 0)),
            pl.BlockSpec((kw, tile), lambda i: (0, i)),
            pl.BlockSpec((tile, pw), lambda i: (i, 0)),
            pl.BlockSpec((1, 8, pw), lambda i: (i, 0, 0)),
            pl.BlockSpec((1, pw), lambda i: (0, 0)),
        ],
        out_shape=[
            jax.ShapeDtypeStruct((length, qw), BF),
            jax.ShapeDtypeStruct((length, 2 * kw), BF),
            jax.ShapeDtypeStruct((kw, length), BF),
            jax.ShapeDtypeStruct((length, pw), BF),
            jax.ShapeDtypeStruct((steps, 8, pw), F32),
            jax.ShapeDtypeStruct((1, pw), F32),
        ],
        compiler_params=pltpu.CompilerParams(
            dimension_semantics=("arbitrary",), vmem_limit_bytes=VMEM
        ),
        cost_estimate=pl.CostEstimate(
            flops=2 * length * width * (qw + 2 * kw + pw),
            bytes_accessed=2 * length * width, transcendentals=0,
        ),
        name="project",
    )(tokens, gain, wq, wk, wv, wp)


def mix_kernel(
    mine, scal, q, kc, kp, vc, vp, pc, pp, khalo, vhalo, phalo, totals, bsum, wg, sinks, *outs
):
    out, logs = outs[-2:]
    step = pl.program_id(0)
    tp, sp, steps = scal[0], scal[1], scal[2]
    half = tp if mine else 1 - tp
    earlier = jnp.sum(totals[...], axis=0)
    first_step = half * pl.num_programs(0) + step
    tile = q.shape[0]
    at_start = first_step == 0
    keys = jnp.concatenate([jnp.where(at_start, khalo[...], kp[...]), kc[...]], axis=0)
    vals = jnp.concatenate([jnp.where(at_start, vhalo[...], vp[...]), vc[...]], axis=1)
    padded = jnp.concatenate(
        [jnp.zeros((WINDOW - phalo.shape[0], phalo.shape[1]), BF), phalo[...]], axis=0
    )
    rows = jnp.concatenate([jnp.where(at_start, padded, pp[...]), pc[...]], axis=0)
    lane = lax.broadcasted_iota(jnp.int32, (WINDOW, WINDOW), 1)
    low = (lane < HEAD_SIZE).astype(F32).astype(BF)
    high = (lane >= HEAD_SIZE).astype(F32).astype(BF)
    heads = 4
    key_id = lax.broadcasted_iota(jnp.int32, (WINDOW, heads * WINDOW), 0)
    query_id = lax.broadcasted_iota(jnp.int32, (WINDOW, heads * WINDOW), 1) % WINDOW
    seen = key_id <= query_id
    seen_f = seen.astype(F32).astype(BF)
    past_f = (key_id > query_id).astype(F32).astype(BF)
    nopast = jnp.logical_and(at_start, sp == 0)
    groups = wg.shape[0]
    drow = lax.broadcasted_iota(jnp.int32, (WINDOW, 2 * WINDOW), 0)
    dist = drow + WINDOW - lax.broadcasted_iota(jnp.int32, (WINDOW, 2 * WINDOW), 1)
    prefix = jnp.logical_and(dist >= 0, dist <= drow).astype(F32).astype(BF)
    blocks_per_sum = scal[3]
    sum_id = lax.broadcasted_iota(jnp.int32, bsum.shape, 0) * blocks_per_sum + (
        lax.broadcasted_iota(jnp.int32, bsum.shape, 1)
    )
    kvs = kc.shape[1] // WINDOW
    nblocks = tile // WINDOW
    sink_rows = [
        jnp.concatenate(
            [jnp.full((1, WINDOW), sinks[kv * heads + h], F32) for h in range(heads)], axis=1
        )
        for kv in range(kvs)
    ]

    def score(b, kv):
        parts = []
        for pair in range(2):
            c = (kv * 2 + pair) * WINDOW
            qp = q[b * WINDOW : (b + 1) * WINDOW, c : c + WINDOW]
            parts += [qp * low, qp * high]
        wr = slice(b * WINDOW, (b + 2) * WINDOW)
        return dot(
            keys[wr, kv * WINDOW : (kv + 1) * WINDOW], jnp.concatenate(parts, axis=0), ((1,), (1,))
        )

    def attend(b, kv, scores):
        br = slice(b * WINDOW, (b + 1) * WINDOW)
        past = scores[:WINDOW]
        if b == 0:
            past = past + jnp.where(nopast, F32(NEG), F32(0))
        picked = jnp.where(seen, scores[WINDOW:], past)
        sink = sink_rows[kv]
        row_max = jnp.maximum(jnp.max(picked, axis=0, keepdims=True), sink)
        weights = jnp.exp(picked - row_max)
        weight_sum = jnp.sum(weights, axis=0, keepdims=True) + jnp.exp(sink - row_max)
        log_row = row_max + jnp.log(weight_sum)
        for h in range(heads):
            logs[kv * heads + h : kv * heads + h + 1, br] = log_row[:, h * WINDOW : (h + 1) * WINDOW]
        wb = weights.astype(BF)
        stacked = jnp.concatenate([wb * past_f, wb * seen_f], axis=0)
        return stacked, 1.0 / weight_sum

    def collect(b, kv, stacked, scale):
        wr = slice(b * WINDOW, (b + 2) * WINDOW)
        o = dot(vals[kv * HEAD_SIZE : (kv + 1) * HEAD_SIZE, wr], stacked) * scale
        o = jnp.concatenate([o[:, h * WINDOW : (h + 1) * WINDOW] for h in range(heads)], axis=0)
        width = heads * HEAD_SIZE
        out[1, b * WINDOW : (b + 1) * WINDOW, kv * width : (kv + 1) * width] = o.astype(BF).T

    sum_row = lax.broadcasted_iota(jnp.int32, bsum.shape, 1)

    def pool_block(b, g):
        br = slice(b * WINDOW, (b + 1) * WINDOW)
        wr = slice(b * WINDOW, (b + 2) * WINDOW)
        cols = slice(g * GDIM, (g + 1) * GDIM)
        block = first_step * nblocks + b
        counted = jnp.logical_and(sum_id < block, sum_row < blocks_per_sum)[:, :, cols]
        carry = earlier[:, cols] + jnp.sum(
            jnp.sum(jnp.where(counted, bsum[:, :, cols], 0.0), axis=0), axis=0, keepdims=True
        )
        position = (
            sp * steps * tile + block * WINDOW
            + lax.broadcasted_iota(jnp.int32, (WINDOW, 1), 0) + 1
        )
        inv_pos = 1.0 / position.astype(F32)
        span = jnp.left_shift(jnp.int32(2), tp * groups + g)
        band = jnp.logical_and(dist >= 0, dist < span).astype(F32).astype(BF)
        sums = dot(jnp.concatenate([prefix, band], axis=0), rows[wr, cols])
        inv_count = 1.0 / jnp.minimum(position, span).astype(F32)
        pooled = (sums[WINDOW:] * inv_count - (sums[:WINDOW] + carry) * inv_pos).astype(BF)
        out[0, br, cols] = dot(pooled, wg[g]).astype(BF)

    units = [(b, kv) for b in range(nblocks) for kv in range(kvs)]
    pools = [(b, g) for b in range(nblocks) for g in range(groups)]
    scores = score(*units[0])
    pending = None
    for u, unit in enumerate(units):
        later = score(*units[u + 1]) if u + 1 < len(units) else None
        if pending is not None:
            collect(*pending)
        if u < len(pools):
            pool_block(*pools[u])
        pending = (*unit, *attend(*unit, scores))
        scores = later
    collect(*pending)
    for extra in pools[len(units) :]:
        pool_block(*extra)


def mix(mine, scal, q, kd, vt, pool, khalo, vhalo, phalo, totals, bsum, wg, sinks, *logs_in):
    length, qw = q.shape
    tile = 256
    per = tile // WINDOW
    steps = length // tile // 2
    pw = pool.shape[1]
    heads = sinks.shape[0]
    half = lambda s: s[0] if mine else 1 - s[0]
    cur = lambda i, s: half(s) * steps + i
    prev = lambda i, s: jnp.maximum(cur(i, s) * per - 1, 0)
    whole = lambda a: pl.BlockSpec(a.shape, lambda i, s: (0,) * a.ndim)
    return pl.pallas_call(
        functools.partial(mix_kernel, mine),
        grid_spec=pltpu.PrefetchScalarGridSpec(
            num_scalar_prefetch=1,
            grid=(steps,),
            in_specs=[
                pl.BlockSpec((tile, qw), lambda i, s: (cur(i, s), 0)),
                pl.BlockSpec((tile, kd.shape[1]), lambda i, s: (cur(i, s), 0)),
                pl.BlockSpec((WINDOW, kd.shape[1]), lambda i, s: (prev(i, s), 0)),
                pl.BlockSpec((vt.shape[0], tile), lambda i, s: (0, cur(i, s))),
                pl.BlockSpec((vt.shape[0], WINDOW), lambda i, s: (0, prev(i, s))),
                pl.BlockSpec((tile, pw), lambda i, s: (cur(i, s), 0)),
                pl.BlockSpec((WINDOW, pw), lambda i, s: (prev(i, s), 0)),
                whole(khalo), whole(vhalo), whole(phalo), whole(totals), whole(bsum), whole(wg),
                pl.BlockSpec(memory_space=pltpu.SMEM),
            ]
            + [pl.BlockSpec(memory_space=pl.ANY)] * len(logs_in),
            out_specs=[
                pl.BlockSpec((2, tile, qw), lambda i, s: (0, i, 0)),
                pl.BlockSpec((heads, tile), lambda i, s: (0, cur(i, s))),
            ],
        ),
        out_shape=[
            jax.ShapeDtypeStruct((2, length // 2, qw), BF),
            jax.ShapeDtypeStruct((heads, length), F32),
        ],
        input_output_aliases={15: 1} if logs_in else {},
        compiler_params=pltpu.CompilerParams(
            dimension_semantics=("arbitrary",), vmem_limit_bytes=VMEM
        ),
        cost_estimate=pl.CostEstimate(
            flops=length // 2 * 2 * qw * 1024, bytes_accessed=length * qw * 4,
            transcendentals=length // 2 * 1024,
        ),
        name="mix",
    )(scal, q, kd, kd, vt, vt, pool, pool, khalo, vhalo, phalo, totals, bsum, wg, sinks, *logs_in)


def share_kernel(count, kd, vt, pool, total, khalo, vhalo, phalo, totals, send, recv, tsend, trecv):
    me = lax.axis_index("sp")
    length = kd.shape[0]
    totals[...] = jnp.zeros_like(totals)
    barrier = pltpu.get_barrier_semaphore()
    for hop in range(1, count):
        pl.semaphore_signal(
            barrier, inc=1, device_id={"sp": lax.rem(me + hop, count)}, device_id_type=MESH
        )
    first = me == 0

    @pl.when(first)
    def _():
        khalo[...] = jnp.zeros_like(khalo)
        vhalo[...] = jnp.zeros_like(vhalo)
        phalo[...] = jnp.zeros_like(phalo)

    pl.semaphore_wait(barrier, count - 1)
    right = {"sp": lax.rem(me + 1, count)}
    pairs = (
        (kd.at[pl.ds(length - WINDOW, WINDOW), :], khalo),
        (vt.at[:, pl.ds(length - WINDOW, WINDOW)], vhalo),
        (pool.at[pl.ds(length - 16, 16), :], phalo),
    )
    halos = [
        pltpu.make_async_remote_copy(
            src_ref=src, dst_ref=dst, send_sem=send.at[j], recv_sem=recv.at[j],
            device_id=right, device_id_type=MESH,
        )
        for j, (src, dst) in enumerate(pairs)
    ]

    def sum_copy(hop):
        return pltpu.make_async_remote_copy(
            src_ref=total, dst_ref=totals.at[hop], send_sem=tsend.at[hop],
            recv_sem=trecv.at[hop], device_id={"sp": lax.rem(me + hop, count)},
            device_id_type=MESH,
        )

    @pl.when(me < count - 1)
    def _():
        for copy in halos:
            copy.start()

    for hop in range(1, count):

        @pl.when(me + hop < count)
        def _():
            sum_copy(hop).start()

    @pl.when(me > 0)
    def _():
        for copy in halos:
            copy.wait_recv()

    @pl.when(me < count - 1)
    def _():
        for copy in halos:
            copy.wait_send()

    for hop in range(1, count):

        @pl.when(me >= hop)
        def _():
            sum_copy(hop).wait_recv()

        @pl.when(me + hop < count)
        def _():
            sum_copy(hop).wait_send()


def share(kd, vt, pool, total):
    count = lax.axis_size("sp")
    vmem = pl.BlockSpec(memory_space=pltpu.VMEM)
    return pl.pallas_call(
        functools.partial(share_kernel, count),
        in_specs=[pl.BlockSpec(memory_space=pl.ANY)] * 3 + [vmem],
        out_specs=[vmem] * 4,
        out_shape=[
            jax.ShapeDtypeStruct((WINDOW, kd.shape[1]), BF),
            jax.ShapeDtypeStruct((vt.shape[0], WINDOW), BF),
            jax.ShapeDtypeStruct((16, pool.shape[1]), BF),
            jax.ShapeDtypeStruct((count, *total.shape), F32),
        ],
        scratch_shapes=[
            pltpu.SemaphoreType.DMA((3,)),
            pltpu.SemaphoreType.DMA((3,)),
            pltpu.SemaphoreType.DMA((count,)),
            pltpu.SemaphoreType.DMA((count,)),
        ],
        compiler_params=pltpu.CompilerParams(
            collective_id=0, has_side_effects=True, vmem_limit_bytes=VMEM
        ),
        name="share",
    )(kd, vt, pool, total)


def output_kernel(own, other, w, out, joined, sems):
    width = own.shape[2]

    @pl.when(pl.program_id(0) == 0)
    def _():
        tp = lax.axis_index("tp")
        copies = []
        for kind in range(2):
            for j, (x, who) in enumerate(((own, tp), (other, 1 - tp))):
                start = pl.multiple_of((kind * 2 + who) * width, width)
                copies.append(
                    pltpu.make_async_copy(
                        x.at[kind], joined.at[:, pl.ds(start, width)], sems.at[kind * 2 + j]
                    )
                )
        for copy in copies:
            copy.start()
        for copy in copies:
            copy.wait()

    out[...] = dot(joined[...], w[...]).astype(BF)


def output(own, other, w):
    rows = own.shape[1]
    depth, cols = w.shape
    tile = 512
    return pl.pallas_call(
        output_kernel,
        grid=(cols // tile,),
        in_specs=[
            pl.BlockSpec(memory_space=pl.ANY),
            pl.BlockSpec(memory_space=pl.ANY),
            pl.BlockSpec((depth, tile), lambda i: (0, i)),
        ],
        out_specs=pl.BlockSpec((rows, tile), lambda i: (0, i)),
        out_shape=jax.ShapeDtypeStruct((rows, cols), BF),
        scratch_shapes=[pltpu.VMEM((rows, depth), BF), pltpu.SemaphoreType.DMA((4,))],
        compiler_params=pltpu.CompilerParams(
            dimension_semantics=("arbitrary",), vmem_limit_bytes=VMEM
        ),
        cost_estimate=pl.CostEstimate(
            flops=2 * rows * depth * cols, bytes_accessed=2 * w.size, transcendentals=0
        ),
        name="output",
    )(own, other, w)


def body(tokens, norm_gain, w_query, w_key, w_value, w_pool, w_group, w_out, sinks):
    q, kd, vt, pool, bsum, total = project(
        tokens[0], norm_gain[None, :], w_query, w_key, w_value, w_pool
    )
    length = q.shape[0]
    halos = share(kd, vt, pool, total)
    per_sum = length // bsum.shape[0] // WINDOW
    scal = jnp.stack(
        [lax.axis_index("tp"), lax.axis_index("sp"), jnp.int32(length // 256), jnp.int32(per_sum)]
    ).astype(jnp.int32)
    shared = (scal, q, kd, vt, pool, *halos, bsum, w_group, sinks)
    theirs, logs = mix(False, *shared)
    other = lax.ppermute(theirs, "tp", [(0, 1), (1, 0)])
    own, logs = mix(True, *shared, logs)
    return (output(own, other, w_out)[None], logs[None])


def solution(mesh):
    return jax.shard_map(
        body,
        mesh=mesh,
        in_specs=(
            P("fs", "sp", None),
            P(),
            P(None, "tp"),
            P(None, "tp"),
            P(None, "tp"),
            P(None, "tp"),
            P("tp", None, None),
            P(),
            P("tp"),
        ),
        out_specs=(P("fs", ("sp", "tp"), None), P("fs", "tp", "sp")),
        check_vma=False,
    )
```

profile of v0, /device:TPU:9, one launch (start us, length us, event | category | flops | bytes accessed | tf_op | source)
XLA Modules:
  0.0 65.7 jit_solution(4744575068777697888)
XLA Ops:
  0.6 0.6 pad_add_fusion.scal
  1.2 21.4 %project.1 = (bf16[2048,512]{1,0:T(8,128)(2,1)}, bf16[2048,256]{1,0:T(8,128)(2,1)}, bf16[128,2048]{1,0:T(8,128)(2,1)}, bf16[2048,512]{1,0:T(8,128)(2,1)}, f32[4,8,512]{2,1,0:T(8,128)}, /*index=5*/f32[1,512]{1,0:T(1,128)}) custom-call(bf16[2048,2048]{1,0:T(8,128)(2,1)} %bitcast.7, f32[1,2048]{1,0:T(1,128)} %bitcast.8, bf16[2048,512]{1,0:T(8,128)(2,1)} %wq.1, ...), custom_call_target="tpu_custom_call" | custom-call | flops 10737418240 | bytes 8388608 | tf_op jit(solution)/shard_map/project/pallas_call | solution.py:69
  22.7 7.8 %share.1 = (bf16[128,256]{1,0:T(8,128)(2,1)}, bf16[128,128]{1,0:T(8,128)(2,1)}, bf16[16,512]{1,0:T(8,128)(2,1)}, f32[4,1,512]{2,1,0:T(1,128)}) custom-call(bf16[2048,256]{1,0:T(8,128)(2,1)} %get-tuple-element.17.kd.kc.kp, bf16[128,2048]{1,0:T(8,128)(2,1)} %get-tuple-element.18.vt.vc.vp, bf16[2048,512]{1,0:T(8,128)(2,1)} %get-tuple-element.19.pool.pc.pp, ...), custom_call_target="tpu_custom_call" | custom-call | tf_op jit(solution)/shard_map/share/pallas_call | solution.py:345
  30.5 9.7 %mix.2 = (bf16[2,1024,512]{2,1,0:T(8,128)(2,1)}, f32[8,2048]{1,0:T(8,128)}) custom-call(s32[4]{0:T(128)} %pad_add_fusion.scal, bf16[2048,512]{1,0:T(8,128)(2,1)} %get-tuple-element.16.q, bf16[2048,256]{1,0:T(8,128)(2,1)} %get-tuple-element.17.kd.kc.kp, bf16[2048,256]{1,0:T(8,128)(2,1)} %get-tuple-element.17.kd.kc.kp, ...), custom_call_target="tpu_custom_call" | custom-call | flops 1073741824 | bytes 4194304 | tf_op jit(solution)/shard_map/mix/pallas_call | solution.py:233
  40.2 1.6 %collective-permute-start = (bf16[2,1024,512]{2,1,0:T(8,128)(2,1)}, bf16[2,1024,512]{2,1,0:T(8,128)(2,1)}, u32[]{:S(2)}, u32[]{:S(2)}) collective-permute-start(bf16[2,1024,512]{2,1,0:T(8,128)(2,1)} %get-tuple-element.28), channel_id=1, source_target_pairs={{0,1},{1,0},{2,3},{3,2},{4,5},{5,4},{6,7},{7,6},{8,9},{9,8},{10,11... | collective-permute-start | bytes 6291464 | tf_op jit(solution)/shard_map/ppermute | solution.py:428
  41.8 9.6 %mix.3 = (bf16[2,1024,512]{2,1,0:T(8,128)(2,1)}, f32[8,2048]{1,0:T(8,128)}) custom-call(s32[4]{0:T(128)} %pad_add_fusion.scal, bf16[2048,512]{1,0:T(8,128)(2,1)} %get-tuple-element.16.q, bf16[2048,256]{1,0:T(8,128)(2,1)} %get-tuple-element.17.kd.kc.kp, bf16[2048,256]{1,0:T(8,128)(2,1)} %get-tuple-element.17.kd.kc.kp, ...), custom_call_target="tpu_custom_call", output_to_operand_aliasing={{1}: (15, {})} | custom-call | flops 1073741824 | bytes 4194304 | tf_op jit(solution)/shard_map/mix/pallas_call | solution.py:233
  51.4 0.0 collective-permute-done.other
  51.4 14.3 %output.1 = bf16[1024,2048]{1,0:T(8,128)(2,1)} custom-call(bf16[2,1024,512]{2,1,0:T(8,128)(2,1)} %get-tuple-element.27.own, bf16[2,1024,512]{2,1,0:T(8,128)(2,1)} %collective-permute-done.other, bf16[2048,2048]{1,0:T(8,128)(2,1)} %w.1), custom_call_target="tpu_custom_call" | custom-call | flops 8589934592 | bytes 8388608 | tf_op jit(solution)/shard_map/output/pallas_call | solution.py:395
Async XLA Ops:
  40.2 11.2 %collective-permute-start = (bf16[2,1024,512]{2,1,0:T(8,128)(2,1)}, bf16[2,1024,512]{2,1,0:T(8,128)(2,1)}, u32[]{:S(2)}, u32[]{:S(2)}) collective-permute-start(bf16[2,1024,512]{2,1,0:T(8,128)(2,1)} %get-tuple-element.28), channel_id=1, source_target_pairs={{0,1},{1,0},{2,3},{3,2},{4,5},{5,4},{6,7},{7,6},{8,9},{9,8},{10,11... | collective-permute-start | bytes 6291464 | tf_op jit(solution)/shard_map/ppermute | solution.py:428
where the time goes:
time: 66 us; the launch traced here: 65.7 us
  Pallas kernels  62.9 us (95%)
  starting transfers between devices  1.62 us (2%)
  between operations  0.66 us (1%)
    pallas_call x1, Pallas kernels, project(): pl.pallas_call(functools.partial(project_kernel, tile // SUB), grid=(step...  21.4 us
    pallas_call x2, Pallas kernels, mix(): pl.pallas_call(functools.partial(mix_kernel, mine), grid_spec=pltpu.Prefe...  19.3 us
    pallas_call x1, Pallas kernels, output(): pl.pallas_call(output_kernel, grid=(cols // tile,), in_specs=[pl.BlockSpe...  14.3 us
    pallas_call x1, Pallas kernels, share(): pl.pallas_call(functools.partial(share_kernel, count), in_specs=[pl.Block...  7.8 us
    ppermute x1, starting transfers between devices, body(): other = lax.ppermute(theirs, 'tp', [(0, 1), (1, 0)])  1.62 us
  transfers between devices with their start and end apart: 1, of which 0 were waited for; matrix products, arithmetic and copies ran while one was open for 0% of the time, Pallas kernels for 15%

commit v1 on v0

v1 whole, which is shorter than its diff:
```python
import functools

import jax
import jax.numpy as jnp
from jax import lax
from jax.experimental import pallas as pl
from jax.experimental.pallas import tpu as pltpu
from jax.sharding import PartitionSpec as P

HEAD_SIZE = 64
GDIM = 256
WINDOW = 128
LN_EPS = 1e-05
SUB = 256
HEADS = 4
HALO = 16
MESH = pl.DeviceIdType.MESH
BF = jnp.bfloat16
F32 = jnp.float32
NEG = -1e30


def dot(a, b, dims=((1,), (0,))):
    return lax.dot_general(a, b, (dims, ((), ())), preferred_element_type=F32)


def layer_kernel(
    count,
    tok_in, gain_in, wq_in, wk_in, wv_in, wp_in, wg_in, sinks_in,
    joined, logs,
    tok, gain, w, wg, sinks, norm_a, norm_b, qs, ks, vs, ps, their_attn, their_pool,
    bsum, total, totals, carry, seen_f, past_f, mixers,
    tok_sem, w_sem, small_sem, halo_send, halo_recv, sum_send, sum_recv, tp_send, tp_recv,
):
    me = lax.axis_index("sp")
    tp = lax.axis_index("tp")
    length, width = tok.shape
    tiles = length // SUB
    qw, pw, kw = wq_in.shape[1], wp_in.shape[1], wk_in.shape[1]
    groups = wg.shape[0]
    kvs = kw // HEAD_SIZE
    half_rows = length // 2
    half_blocks = half_rows // WINDOW

    def tok_copy(i):
        t = lax.rem(i + tiles - 1, tiles)
        rows = pl.ds(pl.multiple_of(t * SUB, SUB), SUB)
        return pltpu.make_async_copy(tok_in.at[rows, :], tok.at[rows, :], tok_sem.at[t])

    w_copies = [
        pltpu.make_async_copy(src, w.at[:, pl.ds(at, src.shape[1])], w_sem.at[n])
        for n, (src, at) in enumerate(
            ((wq_in, 0), (wk_in, qw), (wv_in, qw + kw), (wp_in, qw + 2 * kw))
        )
    ]
    small = [
        pltpu.make_async_copy(src, dst, small_sem.at[n])
        for n, (src, dst) in enumerate(((gain_in, gain), (wg_in, wg), (sinks_in, sinks)))
    ]
    tok_copy(0).start()
    small[0].start()
    for copy in w_copies:
        copy.start()
    tok_copy(1).start()
    small[1].start()
    small[2].start()

    totals[...] = jnp.zeros_like(totals)
    ps[: WINDOW - HALO, :] = jnp.zeros((WINDOW - HALO, pw), BF)

    @pl.when(me == 0)
    def _():
        ks[:WINDOW, :] = jnp.zeros((WINDOW, ks.shape[1]), BF)
        vs[:, :WINDOW] = jnp.zeros((vs.shape[0], WINDOW), BF)
        ps[WINDOW - HALO : WINDOW, :] = jnp.zeros((HALO, pw), BF)

    barrier = pltpu.get_barrier_semaphore()
    for hop in range(1, count):
        pl.semaphore_signal(
            barrier, inc=1, device_id={"sp": lax.rem(me + hop, count)}, device_id_type=MESH
        )
    pl.semaphore_signal(barrier, inc=1, device_id={"tp": 1 - tp}, device_id_type=MESH)

    key_id = lax.broadcasted_iota(jnp.int32, (WINDOW, 2 * WINDOW), 0)
    query_id = lax.broadcasted_iota(jnp.int32, (WINDOW, 2 * WINDOW), 1) % WINDOW
    seen_f[...] = (key_id <= query_id).astype(F32).astype(BF)
    past_f[...] = (key_id > query_id).astype(F32).astype(BF)
    drow = lax.broadcasted_iota(jnp.int32, (WINDOW, 2 * WINDOW), 0)
    dist = drow + WINDOW - lax.broadcasted_iota(jnp.int32, (WINDOW, 2 * WINDOW), 1)
    for g in range(groups):
        span = jnp.left_shift(jnp.int32(2), tp * groups + g)
        mixers[g, :WINDOW] = jnp.logical_and(dist >= 0, dist <= drow).astype(F32).astype(BF)
        mixers[g, WINDOW:] = jnp.logical_and(dist >= 0, dist < span).astype(F32).astype(BF)

    def norm_rows(dst, base, r0, rows):
        x = tok[pl.ds(pl.multiple_of(base + r0, rows), rows), :].astype(F32)
        centered = x - jnp.sum(x, axis=-1, keepdims=True) * (1.0 / width)
        variance = jnp.sum(centered * centered, axis=-1, keepdims=True) * (1.0 / width)
        dst[r0 : r0 + rows, :] = (
            centered * lax.rsqrt(variance + LN_EPS) * gain[...]
        ).astype(BF)

    def project_tile(i, src, dst):
        t = lax.rem(i + tiles - 1, tiles)
        base = pl.multiple_of(t * SUB, SUB)
        nxt = pl.multiple_of(lax.rem(i + tiles, tiles) * SUB, SUB)
        rows = pl.ds(base, SUB)
        shifted = pl.ds(base + WINDOW, SUB)
        chunk = 16
        todo = [functools.partial(norm_rows, dst, nxt, r0, chunk) for r0 in range(0, SUB, chunk)]

        def norms(n):
            for _ in range(min(n, len(todo))):
                todo.pop(0)()

        x = src[...]
        norms(3)
        qs[rows, :] = (dot(x, w[:, :qw]) * HEAD_SIZE**-0.5).astype(BF)
        norms(5)
        kv = dot(x, w[:, qw : qw + 2 * kw])
        norms(3)
        p = dot(x, w[:, qw + 2 * kw :]).astype(BF)
        norms(16)
        k = kv[:, :kw]
        lane = lax.broadcasted_iota(jnp.int32, k.shape, 1)
        low = lane < HEAD_SIZE
        rolled = pltpu.roll(k, HEAD_SIZE, 1)
        zero = jnp.zeros_like(k)
        for n, part in enumerate(
            (
                jnp.where(low, k, zero), jnp.where(low, zero, rolled),
                jnp.where(low, rolled, zero), jnp.where(low, zero, k),
            )
        ):
            ks[shifted, n * WINDOW : (n + 1) * WINDOW] = part.astype(BF)
        vs[:, shifted] = kv[:, kw:].T.astype(BF)
        ps[shifted, :] = p
        pf = p.astype(F32)
        for b in range(SUB // WINDOW):
            part = jnp.sum(
                pf[b * WINDOW : (b + 1) * WINDOW].reshape(WINDOW // 8, 8, pw), axis=0
            )
            bsum[t * (SUB // WINDOW) + b] = part

    halo_pairs = (
        (ks.at[pl.ds(length, WINDOW), :], ks.at[pl.ds(0, WINDOW), :]),
        (vs.at[:, pl.ds(length, WINDOW)], vs.at[:, pl.ds(0, WINDOW)]),
        (
            ps.at[pl.ds(length + WINDOW - HALO, HALO), :],
            ps.at[pl.ds(WINDOW - HALO, HALO), :],
        ),
    )
    halos = [
        pltpu.make_async_remote_copy(
            src_ref=src, dst_ref=dst, send_sem=halo_send.at[n], recv_sem=halo_recv.at[n],
            device_id={"sp": lax.rem(me + 1, count)}, device_id_type=MESH,
        )
        for n, (src, dst) in enumerate(halo_pairs)
    ]

    def sum_copy(hop):
        return pltpu.make_async_remote_copy(
            src_ref=total, dst_ref=totals.at[hop], send_sem=sum_send.at[hop],
            recv_sem=sum_recv.at[hop], device_id={"sp": lax.rem(me + hop, count)},
            device_id_type=MESH,
        )

    tok_copy(0).wait()
    small[0].wait()
    for r0 in range(0, SUB, 16):
        norm_rows(norm_a, (tiles - 1) * SUB, r0, 16)
    for copy in w_copies:
        copy.wait()

    def project_pair(j, _):
        i = 2 * j

        @pl.when(j == 1)
        def _():
            pl.semaphore_wait(barrier, count)

            @pl.when(me < count - 1)
            def _():
                for copy in halos:
                    copy.start()

        tok_copy(i + 1).wait()

        @pl.when(i + 2 < tiles)
        def _():
            tok_copy(i + 2).start()
            tok_copy(i + 3).start()

        project_tile(i, norm_a, norm_b)

        @pl.when(i + 2 < tiles)
        def _():
            tok_copy(i + 2).wait()

        project_tile(i + 1, norm_b, norm_a)
        return 0

    lax.fori_loop(0, tiles // 2, project_pair, 0)

    acc = bsum[0]
    for b in range(1, length // WINDOW):
        acc = acc + bsum[b]
    total[...] = acc

    small[1].wait()
    small[2].wait()

    @pl.when(me > 0)
    def _():
        for copy in halos:
            copy.wait_recv()

    @pl.when(me < count - 1)
    def _():
        for copy in halos:
            copy.wait_send()

    for hop in range(1, count):

        @pl.when(me + hop < count)
        def _():
            sum_copy(hop).start()

    def score(block, kv):
        start = pl.multiple_of(block * WINDOW, WINDOW)
        window = pl.ds(start, 2 * WINDOW)
        c = kv * 2 * WINDOW
        rhs = jnp.concatenate(
            [qs[pl.ds(start, WINDOW), c + n * WINDOW : c + (n + 1) * WINDOW] for n in range(2)],
            axis=0,
        )
        lhs = jnp.concatenate(
            [ks[window, c + n * WINDOW : c + (n + 1) * WINDOW] for n in range(2)], axis=0
        )
        return dot(lhs, rhs, ((1,), (1,)))

    def attend(block, kv, scores, penalty):
        cols = pl.ds(pl.multiple_of(block * WINDOW, WINDOW), WINDOW)
        seen = seen_f[...] > 0
        stacked, scales = [], []
        for parity in range(2):
            s = scores[parity * 2 * WINDOW : (parity + 1) * 2 * WINDOW]
            past = s[:WINDOW]
            if penalty is not None:
                past = past + penalty
            picked = jnp.where(seen, s[WINDOW:], past)
            heads = [kv * HEADS + 2 * pair + parity for pair in range(2)]
            sink = jnp.concatenate(
                [jnp.full((1, WINDOW), sinks[h], F32) for h in heads], axis=1
            )
            row_max = jnp.maximum(jnp.max(picked, axis=0, keepdims=True), sink)
            weights = jnp.exp(picked - row_max)
            weight_sum = jnp.sum(weights, axis=0, keepdims=True) + jnp.exp(sink - row_max)
            log_row = row_max + jnp.log(weight_sum)
            for pair in range(2):
                logs[heads[pair] : heads[pair] + 1, cols] = log_row[
                    :, pair * WINDOW : (pair + 1) * WINDOW
                ]
            wb = weights.astype(BF)
            stacked.append(jnp.concatenate([wb * past_f[...], wb * seen_f[...]], axis=0))
            scales.append(1.0 / weight_sum)
        return stacked, scales

    def collect(block, kv, stacked, scales, dest, row, col):
        window = pl.ds(pl.multiple_of(block * WINDOW, WINDOW), 2 * WINDOW)
        v = vs[kv * HEAD_SIZE : (kv + 1) * HEAD_SIZE, window]
        outs = [dot(v, s) * scale for s, scale in zip(stacked, scales)]
        for pair in range(2):
            cols = slice(pair * WINDOW, (pair + 1) * WINDOW)
            o = jnp.concatenate([o[:, cols] for o in outs], axis=0)
            at = col + (kv * 2 + pair) * WINDOW
            if not isinstance(at, int):
                at = pl.multiple_of(at, WINDOW)
            dest[pl.ds(row, WINDOW), pl.ds(at, WINDOW)] = o.astype(BF).T

    def pool_block(block, g, dest, row, col):
        start = pl.multiple_of(block * WINDOW, WINDOW)
        cols = slice(g * GDIM, (g + 1) * GDIM)
        position = (
            me * length + block * WINDOW + 1
            + lax.broadcasted_iota(jnp.int32, (WINDOW, WINDOW), 0)
        )
        span = jnp.left_shift(jnp.int32(2), tp * groups + g)
        inv_pos = 1.0 / position.astype(F32)
        inv_count = 1.0 / jnp.minimum(position, span).astype(F32)
        inv_pos = jnp.concatenate([inv_pos] * (GDIM // WINDOW), axis=1)
        inv_count = jnp.concatenate([inv_count] * (GDIM // WINDOW), axis=1)
        sums = dot(mixers[g], ps[pl.ds(start, 2 * WINDOW), cols])
        before = carry[pl.ds(block, 1), cols]
        pooled = (sums[WINDOW:] * inv_count - (sums[:WINDOW] + before) * inv_pos).astype(BF)
        at = col + g * GDIM
        if not isinstance(at, int):
            at = pl.multiple_of(at, GDIM)
        dest[pl.ds(row, WINDOW), pl.ds(at, GDIM)] = dot(pooled, wg[g]).astype(BF)

    def mix(first, blocks, attn_to, pools):
        dest, row0, col = attn_to
        units = [(b, kv) for b in range(blocks) for kv in range(kvs)]
        nopast = jnp.logical_and(first == 0, me == 0)
        penalty = jnp.where(nopast, F32(NEG), F32(0))
        per = -(-len(pools) // len(units)) if units else 0
        pools = list(pools)

        def where(b):
            return pl.multiple_of(row0 + b * WINDOW, WINDOW)

        scores = score(first + units[0][0], units[0][1])
        pending = None
        for u, (b, kv) in enumerate(units):
            later = None
            if u + 1 < len(units):
                later = score(first + units[u + 1][0], units[u + 1][1])
            if pending is not None:
                collect(*pending)
            for _ in range(min(per, len(pools))):
                pool_block(*pools.pop(0))
            done = attend(first + b, kv, scores, penalty if b == 0 else None)
            pending = (first + b, kv, *done, dest, where(b), col)
            scores = later
        collect(*pending)

    mine, other = tp * half_blocks, (1 - tp) * half_blocks
    step = half_blocks // 2
    attn_col = 2 * pw + tp * qw
    pool_col = tp * pw

    def their_step(j, _):
        mix(other + j * step, step, (their_attn, j * step * WINDOW, 0), ())
        return 0

    lax.fori_loop(0, 2, their_step, 0)

    def tp_copy(n):
        src, col = ((their_attn, attn_col), (their_pool, pool_col))[n]
        return pltpu.make_async_remote_copy(
            src_ref=src,
            dst_ref=joined.at[:, pl.ds(pl.multiple_of(col, 512), src.shape[1])],
            send_sem=tp_send.at[n], recv_sem=tp_recv.at[n],
            device_id={"tp": 1 - tp}, device_id_type=MESH,
        )

    for hop in range(1, count):

        @pl.when(me >= hop)
        def _():
            sum_copy(hop).wait_recv()

        @pl.when(me + hop < count)
        def _():
            sum_copy(hop).wait_send()

    tp_copy(0).start()
    acc = jnp.sum(totals[...], axis=0)
    for b in range(length // WINDOW):
        carry[b : b + 1, :] = jnp.sum(acc, axis=0, keepdims=True)
        acc = acc + bsum[b]

    mix(
        mine, step, (joined, 0, attn_col),
        [(other + b, g, their_pool, b * WINDOW, 0) for b in range(half_blocks) for g in range(groups)],
    )
    tp_copy(1).start()
    mix(
        mine + step, step, (joined, step * WINDOW, attn_col),
        [(mine + b, g, joined, b * WINDOW, pool_col) for b in range(half_blocks) for g in range(groups)],
    )

    for n in range(2):
        src, col = ((their_attn, 2 * pw + (1 - tp) * qw), (their_pool, (1 - tp) * pw))[n]
        tp_copy(n).wait_send()
        tp_copy(n).wait_recv()


def layer(tokens, gain, wq, wk, wv, wp, wg, sinks):
    length, width = tokens.shape
    count = lax.axis_size("sp")
    qw, kw, pw = wq.shape[1], wk.shape[1], wp.shape[1]
    groups = wg.shape[0]
    blocks = length // WINDOW
    heads = sinks.shape[0]
    any_ = pl.BlockSpec(memory_space=pl.ANY)
    vmem = pl.BlockSpec(memory_space=pltpu.VMEM)
    return pl.pallas_call(
        functools.partial(layer_kernel, count),
        in_specs=[any_] * 8,
        out_specs=[vmem, vmem],
        out_shape=[
            pltpu.VMEM((length // 2, 2 * (qw + pw)), BF),
            pltpu.VMEM((heads, length), F32),
        ],
        scratch_shapes=[
            pltpu.VMEM((length, width), BF),
            pltpu.VMEM(gain.shape, F32),
            pltpu.VMEM((width, qw + 2 * kw + pw), BF),
            pltpu.VMEM(wg.shape, BF),
            pltpu.SMEM(sinks.shape, F32),
            pltpu.VMEM((SUB, width), BF),
            pltpu.VMEM((SUB, width), BF),
            pltpu.VMEM((length, qw), BF),
            pltpu.VMEM((length + WINDOW, 4 * kw), BF),
            pltpu.VMEM((kw, length + WINDOW), BF),
            pltpu.VMEM((length + WINDOW, pw), BF),
            pltpu.VMEM((length // 2, qw), BF),
            pltpu.VMEM((length // 2, pw), BF),
            pltpu.VMEM((blocks, 8, pw), F32),
            pltpu.VMEM((8, pw), F32),
            pltpu.VMEM((count, 8, pw), F32),
            pltpu.VMEM((blocks, pw), F32),
            pltpu.VMEM((WINDOW, 2 * WINDOW), BF),
            pltpu.VMEM((WINDOW, 2 * WINDOW), BF),
            pltpu.VMEM((groups, 2 * WINDOW, 2 * WINDOW), BF),
            pltpu.SemaphoreType.DMA((length // SUB,)),
            pltpu.SemaphoreType.DMA((4,)),
            pltpu.SemaphoreType.DMA((3,)),
            pltpu.SemaphoreType.DMA((3,)),
            pltpu.SemaphoreType.DMA((3,)),
            pltpu.SemaphoreType.DMA((count,)),
            pltpu.SemaphoreType.DMA((count,)),
            pltpu.SemaphoreType.DMA((2,)),
            pltpu.SemaphoreType.DMA((2,)),
        ],
        compiler_params=pltpu.CompilerParams(
            collective_id=0, has_side_effects=True, vmem_limit_bytes=40 * 2**20
        ),
        cost_estimate=pl.CostEstimate(
            flops=2 * length * width * (qw + 2 * kw + pw),
            bytes_accessed=2 * length * width, transcendentals=0,
        ),
        name="layer",
    )(tokens, gain, wq, wk, wv, wp, wg, sinks)


def output_kernel(joined, logs_in, w, out, logs):
    @pl.when(pl.program_id(0) == 0)
    def _():
        logs[...] = logs_in[...]

    out[...] = dot(joined[...], w[...]).astype(BF)


def output(joined, logs, w):
    rows = joined.shape[0]
    depth, cols = w.shape
    tile = 256
    vmem = pl.BlockSpec(memory_space=pltpu.VMEM)
    return pl.pallas_call(
        output_kernel,
        grid=(cols // tile,),
        in_specs=[
            vmem,
            vmem,
            pl.BlockSpec((depth, tile), lambda i: (0, i)),
        ],
        out_specs=[
            pl.BlockSpec((rows, tile), lambda i: (0, i)),
            pl.BlockSpec(logs.shape, lambda i: (0, 0)),
        ],
        out_shape=[
            jax.ShapeDtypeStruct((rows, cols), BF),
            jax.ShapeDtypeStruct(logs.shape, F32),
        ],
        compiler_params=pltpu.CompilerParams(
            dimension_semantics=("arbitrary",), vmem_limit_bytes=40 * 2**20
        ),
        cost_estimate=pl.CostEstimate(
            flops=2 * rows * depth * cols, bytes_accessed=2 * w.size, transcendentals=0
        ),
        name="output",
    )(joined, logs, w)


def body(tokens, norm_gain, w_query, w_key, w_value, w_pool, w_group, w_out, sinks):
    joined, logs = layer(
        tokens[0], norm_gain[None, :], w_query, w_key, w_value, w_pool, w_group, sinks
    )
    mixed, logs = output(joined, logs, w_out)
    return (mixed[None], logs[None])


def solution(mesh):
    return jax.shard_map(
        body,
        mesh=mesh,
        in_specs=(
            P("fs", "sp", None),
            P(),
            P(None, "tp"),
            P(None, "tp"),
            P(None, "tp"),
            P(None, "tp"),
            P("tp", None, None),
            P(),
            P("tp"),
        ),
        out_specs=(P("fs", ("sp", "tp"), None), P("fs", "tp", "sp")),
        check_vma=False,
    )
```

time: 66 us -> 48.6 us (0.74)
  Pallas kernels: 62.9 us -> 40 us
  local copies, waits for them, and re-layouts: 0 us -> 7.56 us
  starting transfers between devices: 1.62 us -> 0 us
    pallas_call x5 -> x2, Pallas kernels: 62.9 us -> 40 us  [the longest x1 27.9 us: layer(): pl.pallas_call(functools.partial(layer_kernel, count), in_specs=[any_] *...]
    unnamed x0 -> x16, local copies, waits for them, and re-layouts: none -> 7.56 us
    ppermute x1 -> x0, starting transfers between devices: 1.62 us -> none  [body(): other = lax.ppermute(theirs, 'tp', [(0, 1), (1, 0)])]
  transfers between devices with their start and end apart: 1 -> 0, of which waited for: 0 -> 0; matrix products, arithmetic and copies ran while one was open for 0% -> 0% of each run, Pallas kernels for 15% -> 0%
where the time goes in v1:
time: 48.6 us; the launch traced here: 48.3 us
  Pallas kernels  40 us (82%)
  local copies, waits for them, and re-layouts  7.56 us (16%)
  between operations  0.66 us (1%)
    pallas_call x1, Pallas kernels, layer(): pl.pallas_call(functools.partial(layer_kernel, count), in_specs=[any_] *...  27.9 us
    pallas_call x1, Pallas kernels, output(): pl.pallas_call(output_kernel, grid=(cols // tile,), in_specs=[vmem, vmem,...  12.2 us
    unnamed x16, local copies, waits for them, and re-layouts  7.56 us

profile of v1, /device:TPU:9, one launch (start us, length us, event | category | flops | bytes accessed | tf_op | source)
XLA Modules:
  0.0 48.3 jit_solution(10217771141683338575)
XLA Ops:
  0.6 0.0 copy-start.1
  0.6 1.6 %copy-done.1 = bf16[2048,512]{1,0:T(8,128)(2,1)S(1)} copy-done((bf16[2048,512]{1,0:T(8,128)(2,1)S(1)}, bf16[2048,512]{1,0:T(8,128)(2,1)}, u32[]{:S(2)}) %copy-start.1) | copy-done | bytes 2097176
  2.2 0.0 copy-start.2
  2.2 1.6 %copy-done.2 = bf16[2048,512]{1,0:T(8,128)(2,1)S(1)} copy-done((bf16[2048,512]{1,0:T(8,128)(2,1)S(1)}, bf16[2048,512]{1,0:T(8,128)(2,1)}, u32[]{:S(2)}) %copy-start.2) | copy-done | bytes 2097176
  3.8 0.0 copy-start.3
  3.8 1.0 %copy-done.3 = bf16[2048,128]{1,0:T(8,128)(2,1)S(1)} copy-done((bf16[2048,128]{1,0:T(8,128)(2,1)S(1)}, bf16[2048,128]{1,0:T(8,128)(2,1)}, u32[]{:S(2)}) %copy-start.3) | copy-done | bytes 524312
  4.9 0.0 copy-start.4
  4.9 1.0 %copy-done.4 = bf16[2048,128]{1,0:T(8,128)(2,1)S(1)} copy-done((bf16[2048,128]{1,0:T(8,128)(2,1)S(1)}, bf16[2048,128]{1,0:T(8,128)(2,1)}, u32[]{:S(2)}) %copy-start.4) | copy-done | bytes 524312
  5.9 0.0 copy-start.5
  5.9 0.9 %copy-done.5 = bf16[2,256,256]{2,1,0:T(8,128)(2,1)S(1)} copy-done((bf16[2,256,256]{2,1,0:T(8,128)(2,1)S(1)}, bf16[2,256,256]{2,1,0:T(8,128)(2,1)}, u32[]{:S(2)}) %copy-start.5) | copy-done | bytes 262168
  6.9 0.0 copy-start.6
  6.9 0.7 %copy-done.6 = f32[2048]{0:T(1024)S(1)} copy-done((f32[2048]{0:T(1024)S(1)}, f32[2048]{0:T(1024)}, u32[]{:S(2)}) %copy-start.6) | copy-done | bytes 8216
  7.5 0.0 copy-start.7
  7.6 0.7 %copy-done.7 = f32[8]{0:T(128)S(1)} copy-done((f32[8]{0:T(128)S(1)}, f32[8]{0:T(128)}, u32[]{:S(2)}) %copy-start.7) | copy-done | bytes 56
  8.2 0.0 copy-start
  8.2 27.9 %layer.1 = (bf16[1024,2048]{1,0:T(8,128)(2,1)S(1)}, f32[8,2048]{1,0:T(8,128)S(1)}) custom-call(bf16[2048,2048]{1,0:T(8,128)(2,1)} %bitcast.5, f32[1,2048]{1,0:T(1,128)S(1)} %bitcast.4, bf16[2048,512]{1,0:T(8,128)(2,1)S(1)} %copy-done.1, bf16[2048,128]{1,0:T(8,128)(2,1)S(1)} %copy-done.3, bf16[2048,128]{1,0:T(8,128)(2,1)S(1)} %copy-done.4, ...), custom_call_target="tpu_custom_call" | custom-call | flops 10737418240 | bytes 8388608 | tf_op jit(solution)/shard_map/layer/pallas_call | solution.py:388
  36.1 0.0 copy-done
  36.1 12.2 %output.1 = (bf16[1024,2048]{1,0:T(8,128)(2,1)}, f32[8,2048]{1,0:T(8,128)}) custom-call(bf16[1024,2048]{1,0:T(8,128)(2,1)S(1)} %get-tuple-element.6.joined, f32[8,2048]{1,0:T(8,128)S(1)} %get-tuple-element.7.logs_in, bf16[2048,2048]{1,0:T(8,128)(2,1)S(1)} %copy-done), custom_call_target="tpu_custom_call" | custom-call | flops 8589934592 | bytes 8388608 | tf_op jit(solution)/shard_map/output/pallas_call | solution.py:451
Async XLA Ops:
  0.6 1.6 %copy-start.1 = (bf16[2048,512]{1,0:T(8,128)(2,1)S(1)}, bf16[2048,512]{1,0:T(8,128)(2,1)}, u32[]{:S(2)}) copy-start(bf16[2048,512]{1,0:T(8,128)(2,1)} %wq_in.1) | copy-start | bytes 6291460
  2.2 1.6 %copy-start.2 = (bf16[2048,512]{1,0:T(8,128)(2,1)S(1)}, bf16[2048,512]{1,0:T(8,128)(2,1)}, u32[]{:S(2)}) copy-start(bf16[2048,512]{1,0:T(8,128)(2,1)} %wp_in.1) | copy-start | bytes 6291460
  3.8 1.0 %copy-start.3 = (bf16[2048,128]{1,0:T(8,128)(2,1)S(1)}, bf16[2048,128]{1,0:T(8,128)(2,1)}, u32[]{:S(2)}) copy-start(bf16[2048,128]{1,0:T(8,128)(2,1)} %wk_in.1) | copy-start | bytes 1572868
  4.9 1.0 %copy-start.4 = (bf16[2048,128]{1,0:T(8,128)(2,1)S(1)}, bf16[2048,128]{1,0:T(8,128)(2,1)}, u32[]{:S(2)}) copy-start(bf16[2048,128]{1,0:T(8,128)(2,1)} %wv_in.1) | copy-start | bytes 1572868
  5.9 0.9 %copy-start.5 = (bf16[2,256,256]{2,1,0:T(8,128)(2,1)S(1)}, bf16[2,256,256]{2,1,0:T(8,128)(2,1)}, u32[]{:S(2)}) copy-start(bf16[2,256,256]{2,1,0:T(8,128)(2,1)} %wg_in.1) | copy-start | bytes 786436
  6.9 0.7 %copy-start.6 = (f32[2048]{0:T(1024)S(1)}, f32[2048]{0:T(1024)}, u32[]{:S(2)}) copy-start(f32[2048]{0:T(1024)} %param.10) | copy-start | bytes 24580
  7.5 0.7 %copy-start.7 = (f32[8]{0:T(128)S(1)}, f32[8]{0:T(128)}, u32[]{:S(2)}) copy-start(f32[8]{0:T(128)} %sinks_in.1) | copy-start | bytes 100
  8.2 27.9 %copy-start = (bf16[2048,2048]{1,0:T(8,128)(2,1)S(1)}, bf16[2048,2048]{1,0:T(8,128)(2,1)}, u32[]{:S(2)}) copy-start(bf16[2048,2048]{1,0:T(8,128)(2,1)} %w.1) | copy-start | bytes 25165828
